TPU v7x, 32 devices: a whole 2x2x4 slice. The times are simulated.
32 devices in a mesh: sp: 8 (over z, x), tp: 4 (over y, core).
Axes of the slice: x: 2, y: 2, z: 4, core: 2. Of those that a mesh axis runs over, the one named last changes fastest.
Arguments:
- tokens: bfloat16 [6144, 4096], P('sp', 'tp'), may hold values from -6 to 6
- norm_gain: float32 [4096], replicated, may hold values from 0.1 to 1.9
- w_query: bfloat16 [4096, 2048], P('sp', 'tp'), may hold values from -0.09375 to 0.09375
- w_key: bfloat16 [4096, 1024], P('sp', 'tp'), may hold values from -0.09375 to 0.09375
- w_value: bfloat16 [4096, 1024], P('sp', 'tp'), may hold values from -0.09375 to 0.09375
- w_pool: bfloat16 [4096, 1024], P('sp', 'tp'), may hold values from -0.09375 to 0.09375
- query_gain: float32 [64], replicated, may hold values from 0.5 to 8
- key_gain: float32 [64], replicated, may hold values from 0.5 to 8
- sink_logit: float32 [32], P('tp'), may hold values from 1 to 5
- w_out_pool: bfloat16 [1024, 4096], P('tp', 'sp'), may hold values from -0.75 to 0.75
- w_out_attn: bfloat16 [2048, 4096], P('tp', 'sp'), may hold values from -1.5 to 1.5
Outputs:
- mixed: bfloat16 [6144, 4096], P(('sp', 'tp'))
All inputs are finite; a program needn't handle non-finite values.
Results may differ from a plain program's by a relative error of at most 0.014.
The roundings to bfloat16 on the way count: a program that leaves them out, or rounds other values in their place, can miss the bound.
Values may be sent and summed in bfloat16 or wider, within the bound.
A program may use at most 128 MiB of HBM per device.

v0:
```python
import jax
import jax.numpy as jnp
from jax import lax
from jax.sharding import PartitionSpec as P

HEAD = 64
POOL = 1024
WINDOW = 128
GRID_W = 64
eps = 1e-06
rope_base = 10000.0
neg_big = -1e30
pool_reach = 8


def padded_2(block, sides, width):
    for axis, dim in sides:
        count = lax.axis_size(axis)
        forward = [(i, i + 1) for i in range(count - 1)]
        backward = [(target, source) for source, target in forward]
        low = lax.ppermute(
            lax.slice_in_dim(block, block.shape[dim] - width, None, axis=dim), axis, forward
        )
        high = lax.ppermute(lax.slice_in_dim(block, 0, width, axis=dim), axis, backward)
        block = jnp.concatenate([low, block, high], axis=dim)
    return block


def rope_tables(positions, head_size):
    quarter = head_size // 4
    freqs = 1.0 / rope_base ** (jnp.arange(quarter, dtype=jnp.float32) * 2.0 / (head_size // 2))
    row_angle = (positions // GRID_W).astype(jnp.float32)[:, None] * freqs
    col_angle = (positions % GRID_W).astype(jnp.float32)[:, None] * freqs
    angles = jnp.concatenate([row_angle, row_angle, col_angle, col_angle], axis=-1)
    return (jnp.cos(angles), jnp.sin(angles))


def rotate(heads_in, cosine, sine):
    part_one, part_two, part_three, part_four = jnp.split(heads_in, 4, axis=-1)
    turned = jnp.concatenate([-part_two, part_one, -part_four, part_three], axis=-1)
    return heads_in * cosine[:, None, :] + turned * sine[:, None, :]


def prepare(projected, gain, cosine, sine):
    rows_count = projected.shape[0]
    shaped = projected.reshape(rows_count, -1, HEAD)
    scaled = shaped * lax.rsqrt(jnp.mean(shaped * shaped, axis=-1, keepdims=True) + eps) * gain
    return rotate(scaled, cosine, sine).reshape(rows_count, -1).astype(jnp.bfloat16)


def edge_keys(keys_new, values_new):
    joined = jnp.concatenate([keys_new, values_new], axis=1)
    return padded_2(joined, (("sp", 0),), WINDOW)


def edge_pool(pool_in):
    return padded_2(pool_in, (("sp", 0),), pool_reach)


def window_attention(queries, key_band, sink_logit, positions, seq):
    rows_count = queries.shape[0]
    key_width = key_band.shape[1] // 2
    heads_q = queries.shape[1] // HEAD
    heads_k = key_width // HEAD
    group = heads_q // heads_k
    blocks = rows_count // WINDOW
    stacked = key_band.reshape(blocks + 2, WINDOW, 2 * key_width)
    joined = jnp.concatenate([stacked[:-2], stacked[1:-1], stacked[2:]], axis=1)
    block_keys = joined[:, :, :key_width].reshape(blocks, 3 * WINDOW, heads_k, HEAD)
    block_values = joined[:, :, key_width:].reshape(blocks, 3 * WINDOW, heads_k, HEAD)
    block_queries = queries.reshape(blocks, WINDOW, heads_k, group, HEAD)
    scores = jnp.einsum(
        "nqhgd,nkhd->nhgqk", block_queries, block_keys, preferred_element_type=jnp.float32
    ) * HEAD ** (-0.5)
    query_pos = positions.reshape(blocks, WINDOW)
    key_pos = query_pos[:, :1] - WINDOW + jnp.arange(3 * WINDOW, dtype=jnp.int32)[None, :]
    inside = (
        (jnp.abs(query_pos[:, :, None] - key_pos[:, None, :]) <= WINDOW)
        & (key_pos[:, None, :] >= 0)
        & (key_pos[:, None, :] < seq)
    )
    scores = jnp.where(inside[:, None, None], scores, neg_big)
    sink = sink_logit.reshape(heads_k, group)[None, :, :, None, None]
    top = jnp.maximum(jnp.max(scores, axis=-1, keepdims=True), sink)
    raised = jnp.exp(scores - top)
    totals = jnp.sum(raised, axis=-1, keepdims=True) + jnp.exp(sink - top)
    weights = (raised / totals).astype(jnp.bfloat16)
    result = jnp.einsum(
        "nhgqk,nkhd->nqhgd", weights, block_values, preferred_element_type=jnp.float32
    )
    return result.astype(jnp.bfloat16).reshape(rows_count, heads_q * HEAD)


def window_pool(pool_band, pool_in, positions, seq):
    rows_count = pool_in.shape[0]
    level = lax.axis_index("tp") * pool_in.shape[1] // (POOL // 4)
    padded = pool_band.astype(jnp.float32)
    sum_two = padded[:-1] + padded[1:]
    sum_four = sum_two[:-2] + sum_two[2:]
    sum_eight = sum_four[:-4] + sum_four[4:]
    sum_sixteen = sum_eight[:-8] + sum_eight[8:]
    candidates = jnp.stack(
        [
            sum_two[7 : 7 + rows_count],
            sum_four[6 : 6 + rows_count],
            sum_eight[4 : 4 + rows_count],
            sum_sixteen[:rows_count],
        ]
    )
    chosen = lax.dynamic_index_in_dim(candidates, level, 0, keepdims=False)
    reach = jnp.left_shift(jnp.int32(1), level)
    low = jnp.clip(positions - reach, 0, seq - 1)
    high = jnp.clip(positions + reach - 1, 0, seq - 1)
    counted = (high - low + 1).astype(jnp.float32)
    return (chosen / counted[:, None]).astype(jnp.bfloat16)


def shards(
    tokens,
    norm_gain,
    w_query,
    w_key,
    w_value,
    w_pool,
    query_gain,
    key_gain,
    sink_logit,
    w_out_pool,
    w_out_attn,
):
    gathered = lax.all_gather(tokens, "tp", axis=1, tiled=True)
    rows_count = gathered.shape[0]
    widened = gathered.astype(jnp.float32)
    normed = (
        widened * lax.rsqrt(jnp.mean(widened * widened, axis=1, keepdims=True) + eps) * norm_gain
    ).astype(jnp.bfloat16)
    positions = lax.axis_index("sp") * rows_count + jnp.arange(rows_count, dtype=jnp.int32)
    seq = lax.axis_size("sp") * rows_count
    cosine, sine = rope_tables(positions, HEAD)
    pieces = (
        lax.all_gather(w_query, "sp", axis=0, tiled=True),
        lax.all_gather(w_key, "sp", axis=0, tiled=True),
        lax.all_gather(w_value, "sp", axis=0, tiled=True),
        lax.all_gather(w_pool, "sp", axis=0, tiled=True),
    )
    query_raw, key_raw, value_raw, pool_raw = tuple(
        (jnp.dot(normed, piece, preferred_element_type=jnp.float32) for piece in pieces)
    )
    queries = prepare(query_raw, query_gain, cosine, sine)
    keys_new = prepare(key_raw, key_gain, cosine, sine)
    pool_in = pool_raw.astype(jnp.bfloat16)
    key_band = edge_keys(keys_new, value_raw.astype(jnp.bfloat16))
    pool_band = edge_pool(pool_in)
    pooled = window_pool(pool_band, pool_in, positions, seq)
    attended = window_attention(queries, key_band, sink_logit, positions, seq)
    out_pool, out_attn = (
        lax.all_gather(w_out_pool, "sp", axis=1, tiled=True),
        lax.all_gather(w_out_attn, "sp", axis=1, tiled=True),
    )
    return lax.psum_scatter(
        (
            jnp.dot(pooled, out_pool, preferred_element_type=jnp.float32)
            + jnp.dot(attended, out_attn, preferred_element_type=jnp.float32)
        ).astype(jnp.bfloat16),
        "tp",
        scatter_dimension=0,
        tiled=True,
    )


def solution(mesh):
    placed = (
        P("sp", "tp"),
        P(),
        P("sp", "tp"),
        P("sp", "tp"),
        P("sp", "tp"),
        P("sp", "tp"),
        P(),
        P(),
        P("tp"),
        P("tp", "sp"),
        P("tp", "sp"),
    )
    return jax.shard_map(
        shards, mesh=mesh, in_specs=placed, out_specs=P(("sp", "tp"), None), check_vma=False
    )
```

profile of v0, /device:TPU:0, one launch (start us, length us, event | category | flops | bytes accessed | tf_op | source)
XLA Modules:
  0.0 483.8 jit_solution(7171826045617975616)
XLA Ops:
  12.3 2.8 fusion.11
  15.1 42.9 %all-gather.8.cloned.1.call-done = bf16[768,4096]{1,0:T(8,128)(2,1)} async-done(((bf16[768,1024]{1,0:T(8,128)(2,1)}), bf16[768,4096]{1,0:T(8,128)(2,1)}) %all-gather.8.cloned.1.call-update) | async-done | bytes 6291472 | tf_op jit(solution)/shard_map/all_gather | solution.py:131
  58.0 4.2 fusion
  62.6 5.3 %fusion.2 = bf16[768,4096]{1,0:T(8,128)(2,1)} fusion(bf16[768,4096]{1,0:T(8,128)(2,1)S(1)} %copy-done, f32[4096]{0:T(1024)S(1)} %copy-done.12, f32[768]{0:T(1024)S(1)} %add_rsqrt_fusion.2), kind=kLoop, calls=%fused_computation.4 | loop fusion | flops 12582912 | bytes 12602368 | tf_op jit(solution)/shard_map/convert_element_type | solution.py:136
  68.0 41.3 %all-gather.14.cloned.1.call-done = bf16[4096,256]{1,0:T(8,128)(2,1)} async-done(((bf16[512,256]{1,0:T(8,128)(2,1)}), bf16[4096,256]{1,0:T(8,128)(2,1)}) %all-gather.14.cloned.1.call-update) | async-done | bytes 2097168 | tf_op jit(solution)/shard_map/all_gather | solution.py:142
  109.3 5.3 %multiply_reduce_fusion.1 = (f32[768,4]{0,1:T(4,128)S(1)}, f32[768,256]{0,1:T(8,128)S(1)}) fusion(bf16[768,4096]{1,0:T(8,128)(2,1)} %fusion.2, bf16[4096,256]{1,0:T(8,128)(2,1)} %all-gather.14.cloned.1.call-done), kind=kOutput, calls=%fused_computation.66 | convolution fusion | flops 1611002880 | bytes 9187328 | tf_op jit(solution)/shard_map/dot_general | solution.py:147
  115.0 44.0 %all-gather.16.cloned.1.call-done = bf16[4096,256]{1,0:T(8,128)(2,1)} async-done(((bf16[512,256]{1,0:T(8,128)(2,1)}), bf16[4096,256]{1,0:T(8,128)(2,1)}) %all-gather.16.cloned.1.call-update) | async-done | bytes 2097168 | tf_op jit(solution)/shard_map/all_gather | solution.py:143
  159.0 5.2 %convolution_convert_fusion = bf16[768,256]{0,1:T(8,128)(2,1)S(1)} fusion(bf16[768,4096]{1,0:T(8,128)(2,1)} %fusion.2, bf16[4096,256]{1,0:T(8,128)(2,1)} %all-gather.16.cloned.1.call-done), kind=kOutput, calls=%fused_computation.27 | convolution fusion | flops 1610809344 | bytes 8781824 | tf_op jit(solution)/shard_map/dot_general | solution.py:147
  165.0 3.1 collective-permute-start.2
  168.1 1.5 collective-permute-start.3
  169.6 64.8 %all-gather.18.cloned.1.call-done = bf16[4096,512]{1,0:T(8,128)(2,1)} async-done(((bf16[512,512]{1,0:T(8,128)(2,1)}), bf16[4096,512]{1,0:T(8,128)(2,1)}) %all-gather.18.cloned.1.call-update) | async-done | bytes 4194320 | tf_op jit(solution)/shard_map/all_gather | solution.py:141
  234.4 7.1 %multiply_reduce_fusion = (f32[768,8]{0,1:T(8,128)S(1)}, f32[768,512]{0,1:T(8,128)S(1)}) fusion(bf16[768,4096]{1,0:T(8,128)(2,1)} %fusion.2, bf16[4096,512]{1,0:T(8,128)(2,1)} %all-gather.18.cloned.1.call-done), kind=kOutput, calls=%fused_computation.24 | convolution fusion | flops 3222005760 | bytes 12083200 | tf_op jit(solution)/shard_map/dot_general | solution.py:147
  242.9 41.1 %all-gather.10.cloned.1.call-done = bf16[4096,256]{1,0:T(8,128)(2,1)} async-done(((bf16[512,256]{1,0:T(8,128)(2,1)}), bf16[4096,256]{1,0:T(8,128)(2,1)}) %all-gather.10.cloned.1.call-update) | async-done | bytes 2097168 | tf_op jit(solution)/shard_map/all_gather | solution.py:144
  284.0 5.3 %convolution_convert_fusion.1 = bf16[768,256]{1,0:T(8,128)(2,1)S(1)} fusion(bf16[768,4096]{1,0:T(8,128)(2,1)} %fusion.2, bf16[4096,256]{1,0:T(8,128)(2,1)} %all-gather.10.cloned.1.call-done), kind=kOutput, calls=%fused_computation.28 | convolution fusion | flops 1610809344 | bytes 8781824 | tf_op jit(solution)/shard_map/dot_general | solution.py:147
  289.3 2.5 collective-permute-start
  291.8 1.3 collective-permute-start.1
  294.6 3.4 collective-permute-done.1
  298.4 1.3 fusion.20
  301.0 2.3 pad_maximum_fusion.4
  303.3 1.4 copy.35
  305.0 1.4 copy.34
  306.5 1.2 fusion.45
  307.8 1.7 copy.38
  309.5 1.4 copy.37
  310.9 2.7 fusion.4
  313.7 2.4 fusion.3
  316.3 2.8 fusion.9
  319.6 39.5 %all-gather.20.cloned.1.call-done = bf16[512,4096]{1,0:T(8,128)(2,1)} async-done(((bf16[512,512]{1,0:T(8,128)(2,1)}), bf16[512,4096]{1,0:T(8,128)(2,1)}) %all-gather.20.cloned.1.call-update) | async-done | bytes 4194320 | tf_op jit(solution)/shard_map/all_gather | solution.py:158
  359.1 8.9 %fusion.17 = f32[768,4096]{1,0:T(8,128)} fusion(bf16[512,4096]{1,0:T(8,128)(2,1)} %all-gather.20.cloned.1.call-done, bf16[64,8,6,128]{3,2,1,0:T(8,128)(2,1)S(1)} %bitcast.99), kind=kOutput, calls=%fused_computation.45 | convolution fusion | flops 3221225472 | bytes 17563648 | tf_op jit(solution)/shard_map/dot_general | solution.py:163
  368.0 41.7 %all-gather.12.cloned.1.call-done = bf16[256,4096]{1,0:T(8,128)(2,1)} async-done(((bf16[256,512]{1,0:T(8,128)(2,1)}), bf16[256,4096]{1,0:T(8,128)(2,1)}) %all-gather.12.cloned.1.call-update) | async-done | bytes 2097168 | tf_op jit(solution)/shard_map/all_gather | solution.py:157
  409.7 9.7 %add_convert_fusion = bf16[768,4096]{1,0:T(8,128)(2,1)} fusion(f32[768,4096]{1,0:T(8,128)} %fusion.17, bf16[256,4096]{1,0:T(8,128)(2,1)} %all-gather.12.cloned.1.call-done, s32[]{:T(128)S(6)} %select_n.33, f32[1,768,256]{2,1,0:T(8,128)S(1)} %copy-done.4, f32[1,768,256]{2,1,0:T(8,128)} %get-tuple-element.39, f32[1,768,256]{2,1,0:T(8,128)S(1)} %copy-done.2, ...), kind=kOutput, calls=%fused_computation.5 | convolution fusion | flops 1617887232 | bytes 24120324 | tf_op jit(solution)/shard_map/dot_general | solution.py:162
  419.5 57.4 %reduce-scatter.2.cloned.1.call-done = bf16[192,4096]{1,0:T(8,128)(2,1)} async-done(((bf16[768,4096]{1,0:T(8,128)(2,1)}), bf16[192,4096]{1,0:T(8,128)(2,1)}) %reduce-scatter.2.cloned.1.call-update) | async-done | bytes 1572880 | tf_op jit(solution)/shard_map/reduce_scatter | solution.py:160
  (90 shorter events, 12.8 us)
Async XLA Ops:
  6.5 5.1 %copy-start.13 = (f32[64]{0:T(128)S(1)}, f32[64]{0:T(128)}, u32[]{:S(2)}) copy-start(f32[64]{0:T(128)} %param.18) | copy-start | bytes 772
  6.5 5.2 %copy-start.14 = (f32[64]{0:T(128)S(1)}, f32[64]{0:T(128)}, u32[]{:S(2)}) copy-start(f32[64]{0:T(128)} %param.17) | copy-start | bytes 772
  6.5 5.2 %copy-start.15 = (f32[8]{0:T(128)S(1)}, f32[8]{0:T(128)}, u32[]{:S(2)}) copy-start(f32[8]{0:T(128)} %param.19) | copy-start | bytes 100
  6.5 51.5 %all-gather.8.cloned.1.call-start = ((), (), s32[]{:S(2)}) async-start(), calls=%async_computation.1 | async-start | bytes 7864320 | tf_op jit(solution)/shard_map/all_gather | solution.py:131
  7.3 102.0 %all-gather.14.cloned.1.call-start = ((), (), s32[]{:S(2)}) async-start(), calls=%async_computation.4 | async-start | bytes 2359296 | tf_op jit(solution)/shard_map/all_gather | solution.py:142
  8.0 151.0 %all-gather.16.cloned.1.call-start = ((), (), s32[]{:S(2)}) async-start(), calls=%async_computation.5 | async-start | bytes 2359296 | tf_op jit(solution)/shard_map/all_gather | solution.py:143
  8.7 225.7 %all-gather.18.cloned.1.call-start = ((), (), s32[]{:S(2)}) async-start(), calls=%async_computation.6 | async-start | bytes 4718592 | tf_op jit(solution)/shard_map/all_gather | solution.py:141
  9.3 274.7 %all-gather.10.cloned.1.call-start = ((), (), s32[]{:S(2)}) async-start(), calls=%async_computation.2 | async-start | bytes 2359296 | tf_op jit(solution)/shard_map/all_gather | solution.py:144
  9.9 349.2 %all-gather.20.cloned.1.call-start = ((), (), s32[]{:S(2)}) async-start(), calls=%async_computation.7 | async-start | bytes 4718592 | tf_op jit(solution)/shard_map/all_gather | solution.py:158
  10.5 399.2 %all-gather.12.cloned.1.call-start = ((), (), s32[]{:S(2)}) async-start(), calls=%async_computation.3 | async-start | bytes 2359296 | tf_op jit(solution)/shard_map/all_gather | solution.py:157
  11.2 465.7 %reduce-scatter.2.cloned.1.call-start = ((), (), s32[]{:S(2)}) async-start(), calls=%async_computation.8 | async-start | bytes 7864320 | tf_op jit(solution)/shard_map/reduce_scatter | solution.py:160
  12.3 49.9 %copy-start.12 = (f32[4096]{0:T(1024)S(1)}, f32[4096]{0:T(1024)}, u32[]{:S(2)}) copy-start(f32[4096]{0:T(1024)} %param.12) | copy-start | bytes 49156
  58.0 4.6 copy-start
  164.3 77.3 %copy-start.7 = (bf16[768,256]{0,1:T(8,128)(2,1)}, bf16[768,256]{0,1:T(8,128)(2,1)S(1)}, u32[]{:S(2)}) copy-start(bf16[768,256]{0,1:T(8,128)(2,1)S(1)} %convolution_convert_fusion) | copy-start | bytes 1179652
  165.0 135.9 %collective-permute-start.2 = (bf16[128,512]{0,1:T(8,128)(2,1)}, bf16[128,512]{0,1:T(8,128)(2,1)}, u32[]{:S(2)}, u32[]{:S(2)}) collective-permute-start(bf16[128,512]{0,1:T(8,128)(2,1)} %get-tuple-element.16), channel_id=1, source_target_pairs={{0,4},{4,8},{8,12},{12,16},{16,20},{20,24},{24,28},{1,5},{5,9},{9,... | collective-permute-start | bytes 393224 | tf_op jit(solution)/shard_map/ppermute | solution.py:21
  168.1 132.8 %collective-permute-start.3 = (bf16[128,512]{0,1:T(8,128)(2,1)S(1)}, bf16[128,512]{0,1:T(8,128)(2,1)}, u32[]{:S(2)}, u32[]{:S(2)}) collective-permute-start(bf16[128,512]{0,1:T(8,128)(2,1)S(1)} %get-tuple-element.17), channel_id=1, source_target_pairs={{4,0},{8,4},{12,8},{16,12},{20,16},{24,20},{28,24},{5,1},{9,5},{13... | collective-permute-start | bytes 393224 | tf_op jit(solution)/shard_map/ppermute | solution.py:24
  284.0 9.1 %copy-start.5 = (f32[768,8,16]{0,2,1:T(8,128)S(1)}, f32[768,8,16]{0,2,1:T(8,128)}, u32[]{:S(2)}) copy-start(f32[768,8,16]{0,2,1:T(8,128)} %get-tuple-element.9) | copy-start | bytes 1179652
  284.0 9.1 %copy-start.6 = (f32[768,8,16]{0,2,1:T(8,128)S(1)}, f32[768,8,16]{0,2,1:T(8,128)}, u32[]{:S(2)}) copy-start(f32[768,8,16]{0,2,1:T(8,128)} %get-tuple-element.10) | copy-start | bytes 1179652
  289.3 3.8 copy-start.10
  289.3 5.2 %collective-permute-start = (bf16[8,256]{1,0:T(8,128)(2,1)S(1)}, bf16[8,256]{1,0:T(8,128)(2,1)S(1)}, u32[]{:S(2)}, u32[]{:S(2)}) collective-permute-start(bf16[8,256]{1,0:T(8,128)(2,1)S(1)} %get-tuple-element.22), channel_id=1, source_target_pairs={{0,4},{4,8},{8,12},{12,16},{16,20},{20,24},{24,28},{1,5},{5,9},{9,... | collective-permute-start | bytes 12296 | tf_op jit(solution)/shard_map/ppermute | solution.py:21
  291.8 6.1 %collective-permute-start.1 = (bf16[8,256]{1,0:T(8,128)(2,1)S(1)}, bf16[8,256]{1,0:T(8,128)(2,1)S(1)}, u32[]{:S(2)}, u32[]{:S(2)}) collective-permute-start(bf16[8,256]{1,0:T(8,128)(2,1)S(1)} %get-tuple-element.23), channel_id=1, source_target_pairs={{4,0},{8,4},{12,8},{16,12},{20,16},{24,20},{28,24},{5,1},{9,5},{13... | collective-permute-start | bytes 12296 | tf_op jit(solution)/shard_map/ppermute | solution.py:24
  293.3 4.7 copy-start.11
  299.7 1.2 copy-start.8
  310.9 2.8 copy-start.1
  313.7 2.5 copy-start.9
  359.1 50.6 %copy-start.2 = (f32[1,768,256]{2,1,0:T(8,128)S(1)}, f32[1,768,256]{2,1,0:T(8,128)}, u32[]{:S(2)}) copy-start(f32[1,768,256]{2,1,0:T(8,128)} %get-tuple-element.40) | copy-start | bytes 2359300
  359.1 50.6 %copy-start.3 = (f32[1,768,256]{2,1,0:T(8,128)S(1)}, f32[1,768,256]{2,1,0:T(8,128)}, u32[]{:S(2)}) copy-start(f32[1,768,256]{2,1,0:T(8,128)} %get-tuple-element.41) | copy-start | bytes 2359300
  359.1 50.6 %copy-start.4 = (f32[1,768,256]{2,1,0:T(8,128)S(1)}, f32[1,768,256]{2,1,0:T(8,128)}, u32[]{:S(2)}) copy-start(f32[1,768,256]{2,1,0:T(8,128)} %get-tuple-element.38) | copy-start | bytes 2359300
Sparse Core Ops, SparseCore 0:
  8.9 49.0 all-gather.7
  60.1 49.0 all-gather.13
  111.4 47.6 all-gather.15
  161.0 73.3 all-gather.17
  236.4 47.6 all-gather.9
  285.9 73.1 all-gather.19
  361.2 48.5 all-gather.11
  419.6 57.2 reduce-scatter.1
where the time goes:
time: 484 us
  waiting for transfers between devices  381 us (79%)
  matrix products  47 us (10%)
  other arithmetic  22.8 us (5%)
  between operations  13.9 us (3%)
  local copies, waits for them, and re-layouts  10.9 us (2%)
  starting transfers between devices  8.59 us (2%)
    all_gather x1, waiting for transfers between devices, shards(): lax.all_gather(w_query, 'sp', axis=0, tiled=True)  64.8 us
    reduce_scatter x1, waiting for transfers between devices, shards(): lax.psum_scatter((jnp.dot(pooled, out_pool, preferred_element_type=jnp.fl...  57.4 us
    all_gather x1, waiting for transfers between devices, shards(): lax.all_gather(w_value, 'sp', axis=0, tiled=True)  44 us
    all_gather x1, waiting for transfers between devices, shards(): gathered = lax.all_gather(tokens, 'tp', axis=1, tiled=True)  42.9 us
    all_gather x1, waiting for transfers between devices, shards(): lax.all_gather(w_out_pool, 'sp', axis=1, tiled=True)  41.7 us
    all_gather x1, waiting for transfers between devices, shards(): lax.all_gather(w_key, 'sp', axis=0, tiled=True)  41.3 us
    all_gather x1, waiting for transfers between devices, shards(): lax.all_gather(w_pool, 'sp', axis=0, tiled=True)  41.1 us
    all_gather x1, waiting for transfers between devices, shards(): lax.all_gather(w_out_attn, 'sp', axis=1, tiled=True)  39.5 us
  transfers between devices with their start and end apart: 12, of which 9 were waited for; matrix products, arithmetic and copies ran while one was open for 15% of the time, Pallas kernels for 0%

commit v1 on v0

--- a/solution.py
+++ b/solution.py
@@ -128,7 +128,12 @@
     w_out_pool,
     w_out_attn,
 ):
-    gathered = lax.all_gather(tokens, "tp", axis=1, tiled=True)
+    ring = [tokens]
+    for hop in range(3):
+        ring.append(lax.ppermute(ring[-1], "tp", [(dev, (dev + 1) % 4) for dev in range(4)]))
+    gathered = jnp.roll(
+        jnp.concatenate(ring[::-1], axis=1), (lax.axis_index("tp") + 1) * ring[0].shape[1], axis=1
+    )
     rows_count = gathered.shape[0]
     widened = gathered.astype(jnp.float32)
     normed = (

time: 484 us -> 436 us (0.901)
  waiting for transfers between devices: 381 us -> 339 us
  other arithmetic: 22.8 us -> 10.8 us
    ppermute x0 -> x3, waiting for transfers between devices: none -> 54.1 us  [shards(): lax.ppermute(ring[-1], 'tp', [(dev, (dev + 1) % 4) for dev in range(4)])]
    all_gather x1 -> x0, waiting for transfers between devices: 42.9 us -> none  [shards(): gathered = lax.all_gather(tokens, 'tp', axis=1, tiled=True)]
    all_gather x1, waiting for transfers between devices: 41.1 us -> 0.02 us  [shards(): lax.all_gather(w_pool, 'sp', axis=0, tiled=True)]
    all_gather x1, waiting for transfers between devices: 41.3 us -> 22.8 us  [shards(): lax.all_gather(w_key, 'sp', axis=0, tiled=True)]
    all_gather x1, waiting for transfers between devices: 39.5 us -> 57 us  [shards(): lax.all_gather(w_out_attn, 'sp', axis=1, tiled=True)]
    all_gather x1, waiting for transfers between devices: 64.8 us -> 52.7 us  [shards(): lax.all_gather(w_query, 'sp', axis=0, tiled=True)]
    unnamed x32 -> x39, local copies, waits for them, and re-layouts: 0.42 us -> 6.03 us
    convert_element_type x1 -> x0, other arithmetic: 5.35 us -> none  [shards(): normed = (widened * lax.rsqrt(jnp.mean(widened * widened, axis=1, keepdim...]
  transfers between devices with their start and end apart: 12 -> 14, of which waited for: 9 -> 11; matrix products, arithmetic and copies ran while one was open for 15% -> 13% of each run, Pallas kernels for 0% -> 0%
where the time goes in v1:
time: 436 us
  waiting for transfers between devices  339 us (78%)
  matrix products  47.6 us (11%)
  local copies, waits for them, and re-layouts  14.6 us (3%)
  between operations  14 us (3%)
  other arithmetic  10.8 us (2%)
  starting transfers between devices  10.1 us (2%)
    reduce_scatter x1, waiting for transfers between devices, shards(): lax.psum_scatter((jnp.dot(pooled, out_pool, preferred_element_type=jnp.fl...  57.4 us
    all_gather x1, waiting for transfers between devices, shards(): lax.all_gather(w_out_attn, 'sp', axis=1, tiled=True)  57 us
    ppermute x3, waiting for transfers between devices, shards(): lax.ppermute(ring[-1], 'tp', [(dev, (dev + 1) % 4) for dev in range(4)])  54.1 us
    all_gather x1, waiting for transfers between devices, shards(): lax.all_gather(w_query, 'sp', axis=0, tiled=True)  52.7 us
    all_gather x1, waiting for transfers between devices, shards(): lax.all_gather(w_value, 'sp', axis=0, tiled=True)  43.7 us
    all_gather x1, waiting for transfers between devices, shards(): lax.all_gather(w_out_pool, 'sp', axis=1, tiled=True)  41.6 us
    dot_general x4, matrix products, shards(): jnp.dot(normed, piece, preferred_element_type=jnp.float32)  24.3 us
    all_gather x1, waiting for transfers between devices, shards(): lax.all_gather(w_key, 'sp', axis=0, tiled=True)  22.8 us
  transfers between devices with their start and end apart: 14, of which 11 were waited for; matrix products, arithmetic and copies ran while one was open for 13% of the time, Pallas kernels for 0%

profile of v1, /device:TPU:0, one launch (start us, length us, event | category | flops | bytes accessed | tf_op | source)
XLA Modules:
  0.0 435.8 jit_solution(5015718878999700573)
XLA Ops:
  10.5 20.3 %collective-permute-done = bf16[768,1024]{1,0:T(8,128)(2,1)S(1)} collective-permute-done((bf16[768,1024]{1,0:T(8,128)(2,1)}, bf16[768,1024]{1,0:T(8,128)(2,1)S(1)}, u32[]{:S(2)}, u32[]{:S(2)}) %collective-permute-start) | collective-permute-done | bytes 1572896 | tf_op jit(solution)/shard_map/ppermute | solution.py:133
  32.4 0.7 max.27
  33.1 17.5 %collective-permute-done.1 = bf16[768,1024]{1,0:T(8,128)(2,1)S(1)} collective-permute-done((bf16[768,1024]{1,0:T(8,128)(2,1)S(1)}, bf16[768,1024]{1,0:T(8,128)(2,1)S(1)}, u32[]{:S(2)}, u32[]{:S(2)}) %collective-permute-start.1) | collective-permute-done | bytes 1572896 | tf_op jit(solution)/shard_map/ppermute | solution.py:133
  51.4 2.7 fusion.11
  54.1 16.3 %collective-permute-done.2 = bf16[768,1024]{1,0:T(8,128)(2,1)S(1)} collective-permute-done((bf16[768,1024]{1,0:T(8,128)(2,1)S(1)}, bf16[768,1024]{1,0:T(8,128)(2,1)S(1)}, u32[]{:S(2)}, u32[]{:S(2)}) %collective-permute-start.2) | collective-permute-done | bytes 1572896 | tf_op jit(solution)/shard_map/ppermute | solution.py:133
  71.7 4.5 %copy-done.1 = bf16[768,8192]{1,0:T(8,128)(2,1)} copy-done((bf16[768,8192]{1,0:T(8,128)(2,1)}, bf16[768,8192]{1,0:T(8,128)(2,1)S(1)}, u32[]{:S(2)}) %copy-start.1) | copy-done | bytes 12582936
  76.2 1.3 fusion
  77.5 5.3 %convolution_convert_fusion.1 = bf16[768,256]{1,0:T(8,128)(2,1)S(1)} fusion(bf16[4096,256]{1,0:T(8,128)(2,1)} %all-gather.7.cloned.1.call-done, f32[4096]{0:T(1024)S(1)} %copy-done.15, f32[768]{0:T(1024)S(1)} %add_rsqrt_fusion.2, bf16[768,8192]{1,0:T(8,128)(2,1)} %copy-done.1, s32[]{:T(128)S(6)} %select_n.45), kind=kOutput, calls=%fused_computation.28 | convolution fusion | flops 1623392256 | bytes 8801284 | tf_op jit(solution)/shard_map/dot_general | solution.py:152
  82.8 4.2 collective-permute-start.3
  87.1 1.3 collective-permute-start.4
  88.4 22.8 %all-gather.11.cloned.1.call-done = bf16[4096,256]{1,0:T(8,128)(2,1)} async-done(((bf16[512,256]{1,0:T(8,128)(2,1)}), bf16[4096,256]{1,0:T(8,128)(2,1)}) %all-gather.11.cloned.1.call-update) | async-done | bytes 2097168 | tf_op jit(solution)/shard_map/all_gather | solution.py:147
  111.1 5.6 %multiply_reduce_fusion.1 = (f32[768,4]{0,1:T(4,128)S(1)}, f32[768,256]{0,1:T(8,128)S(1)}) fusion(bf16[4096,256]{1,0:T(8,128)(2,1)} %all-gather.11.cloned.1.call-done, f32[4096]{0:T(1024)S(1)} %copy-done.15, f32[768]{0:T(1024)S(1)} %add_rsqrt_fusion.2, bf16[768,8192]{1,0:T(8,128)(2,1)} %copy-done.1, s32[]{:T(128)S(6)} %select_n.45), kind=kOutput, calls=%fused_computation.66 | convolution fusion | flops 1623585792 | bytes 9206788 | tf_op jit(solution)/shard_map/dot_general | solution.py:152
  117.3 43.7 %all-gather.13.cloned.1.call-done = bf16[4096,256]{1,0:T(8,128)(2,1)} async-done(((bf16[512,256]{1,0:T(8,128)(2,1)}), bf16[4096,256]{1,0:T(8,128)(2,1)}) %all-gather.13.cloned.1.call-update) | async-done | bytes 2097168 | tf_op jit(solution)/shard_map/all_gather | solution.py:148
  160.9 5.6 %convolution_convert_fusion = bf16[768,256]{0,1:T(8,128)(2,1)S(1)} fusion(bf16[4096,256]{1,0:T(8,128)(2,1)} %all-gather.13.cloned.1.call-done, f32[4096]{0:T(1024)S(1)} %copy-done.15, f32[768]{0:T(1024)S(1)} %add_rsqrt_fusion.2, bf16[768,8192]{1,0:T(8,128)(2,1)} %copy-done.1, s32[]{:T(128)S(6)} %select_n.45), kind=kOutput, calls=%fused_computation.27 | convolution fusion | flops 1623392256 | bytes 8801284 | tf_op jit(solution)/shard_map/dot_general | solution.py:152
  166.6 2.5 collective-permute-start.5
  169.0 1.3 collective-permute-start.6
  170.8 1.3 fusion.20
  172.2 1.3 slice_bitcast_fusion.1
  174.0 5.7 %collective-permute-done.6 = bf16[128,512]{0,1:T(8,128)(2,1)S(1)} collective-permute-done((bf16[128,512]{0,1:T(8,128)(2,1)S(1)}, bf16[128,512]{0,1:T(8,128)(2,1)S(1)}, u32[]{:S(2)}, u32[]{:S(2)}) %collective-permute-start.6) | collective-permute-done | bytes 131104 | tf_op jit(solution)/shard_map/ppermute | solution.py:24
  181.2 0.9 copy.38
  182.1 1.4 copy.37
  183.5 52.7 %all-gather.15.cloned.1.call-done = bf16[4096,512]{1,0:T(8,128)(2,1)} async-done(((bf16[512,512]{1,0:T(8,128)(2,1)}), bf16[4096,512]{1,0:T(8,128)(2,1)}) %all-gather.15.cloned.1.call-update) | async-done | bytes 4194320 | tf_op jit(solution)/shard_map/all_gather | solution.py:146
  236.2 7.8 %multiply_reduce_fusion = (f32[768,8]{0,1:T(8,128)S(1)}, f32[768,512]{0,1:T(8,128)S(1)}) fusion(bf16[4096,512]{1,0:T(8,128)(2,1)} %all-gather.15.cloned.1.call-done, f32[4096]{0:T(1024)} %param.12, f32[768]{0:T(1024)S(1)} %copy-done.12, bf16[768,8192]{1,0:T(8,128)(2,1)} %copy-done.1, s32[]{:T(128)S(6)} %select_n.45), kind=kOutput, calls=%fused_computation.24 | convolution fusion | flops 3234588672 | bytes 12102660 | tf_op jit(solution)/shard_map/dot_general | solution.py:152
  245.5 0.9 reshape.301
  246.4 1.7 fusion.4
  248.2 2.4 fusion.3
  250.7 3.0 fusion.9
  254.3 57.0 %all-gather.17.cloned.1.call-done = bf16[512,4096]{1,0:T(8,128)(2,1)} async-done(((bf16[512,512]{1,0:T(8,128)(2,1)}), bf16[512,4096]{1,0:T(8,128)(2,1)}) %all-gather.17.cloned.1.call-update) | async-done | bytes 4194320 | tf_op jit(solution)/shard_map/all_gather | solution.py:163
  311.3 8.9 %fusion.17 = f32[768,4096]{1,0:T(8,128)} fusion(bf16[512,4096]{1,0:T(8,128)(2,1)} %all-gather.17.cloned.1.call-done, bf16[64,8,6,128]{3,2,1,0:T(8,128)(2,1)S(1)} %bitcast.95), kind=kOutput, calls=%fused_computation.45 | convolution fusion | flops 3221225472 | bytes 17563648 | tf_op jit(solution)/shard_map/dot_general | solution.py:168
  320.2 41.6 %all-gather.9.cloned.1.call-done = bf16[256,4096]{1,0:T(8,128)(2,1)} async-done(((bf16[256,512]{1,0:T(8,128)(2,1)}), bf16[256,4096]{1,0:T(8,128)(2,1)}) %all-gather.9.cloned.1.call-update) | async-done | bytes 2097168 | tf_op jit(solution)/shard_map/all_gather | solution.py:162
  361.7 9.7 %add_convert_fusion = bf16[768,4096]{1,0:T(8,128)(2,1)} fusion(f32[768,4096]{1,0:T(8,128)} %fusion.17, bf16[256,4096]{1,0:T(8,128)(2,1)} %all-gather.9.cloned.1.call-done, s32[]{:T(128)S(6)} %select_n.47, f32[1,768,256]{2,1,0:T(8,128)S(1)} %copy-done.5, f32[1,768,256]{2,1,0:T(8,128)} %get-tuple-element.39, f32[1,768,256]{2,1,0:T(8,128)S(1)} %copy-done.3, ...), kind=kOutput, calls=%fused_computation.5 | convolution fusion | flops 1617887232 | bytes 24120324 | tf_op jit(solution)/shard_map/dot_general | solution.py:167
  371.5 57.4 %reduce-scatter.2.cloned.1.call-done = bf16[192,4096]{1,0:T(8,128)(2,1)} async-done(((bf16[768,4096]{1,0:T(8,128)(2,1)}), bf16[192,4096]{1,0:T(8,128)(2,1)}) %reduce-scatter.2.cloned.1.call-update) | async-done | bytes 1572880 | tf_op jit(solution)/shard_map/reduce_scatter | solution.py:165
  (100 shorter events, 12.4 us)
Async XLA Ops:
  6.5 71.0 %all-gather.7.cloned.1.call-start = ((), (), s32[]{:S(2)}) async-start(), calls=%async_computation.1 | async-start | bytes 2359296 | tf_op jit(solution)/shard_map/all_gather | solution.py:149
  7.3 103.9 %all-gather.11.cloned.1.call-start = ((), (), s32[]{:S(2)}) async-start(), calls=%async_computation.3 | async-start | bytes 2359296 | tf_op jit(solution)/shard_map/all_gather | solution.py:147
  8.0 152.9 %all-gather.13.cloned.1.call-start = ((), (), s32[]{:S(2)}) async-start(), calls=%async_computation.4 | async-start | bytes 2359296 | tf_op jit(solution)/shard_map/all_gather | solution.py:148
  8.7 227.4 %all-gather.15.cloned.1.call-start = ((), (), s32[]{:S(2)}) async-start(), calls=%async_computation.5 | async-start | bytes 4718592 | tf_op jit(solution)/shard_map/all_gather | solution.py:146
  9.3 302.0 %all-gather.17.cloned.1.call-start = ((), (), s32[]{:S(2)}) async-start(), calls=%async_computation.6 | async-start | bytes 4718592 | tf_op jit(solution)/shard_map/all_gather | solution.py:163
  9.9 351.8 %all-gather.9.cloned.1.call-start = ((), (), s32[]{:S(2)}) async-start(), calls=%async_computation.2 | async-start | bytes 2359296 | tf_op jit(solution)/shard_map/all_gather | solution.py:162
  9.9 20.8 %collective-permute-start = (bf16[768,1024]{1,0:T(8,128)(2,1)}, bf16[768,1024]{1,0:T(8,128)(2,1)S(1)}, u32[]{:S(2)}, u32[]{:S(2)}) collective-permute-start(bf16[768,1024]{1,0:T(8,128)(2,1)} %param.11), channel_id=1, source_target_pairs={{0,1},{1,2},{2,3},{3,0},{4,5},{5,6},{6,7},{7,4},{8,9},{9,10},{10,1... | collective-permute-start | bytes 4718600 | tf_op jit(solution)/shard_map/ppermute | solution.py:133
  30.8 19.8 %collective-permute-start.1 = (bf16[768,1024]{1,0:T(8,128)(2,1)S(1)}, bf16[768,1024]{1,0:T(8,128)(2,1)S(1)}, u32[]{:S(2)}, u32[]{:S(2)}) collective-permute-start(bf16[768,1024]{1,0:T(8,128)(2,1)S(1)} %collective-permute-done), channel_id=1, source_target_pairs={{0,1},{1,2},{2,3},{3,0},{4,5},{5,6},{6,7},{7,4},{8,9},{9,10},{10,1... | collective-permute-start | bytes 4718600 | tf_op jit(solution)/shard_map/ppermute | solution.py:133
  30.8 398.1 %reduce-scatter.2.cloned.1.call-start = ((), (), s32[]{:S(2)}) async-start(), calls=%async_computation.7 | async-start | bytes 7864320 | tf_op jit(solution)/shard_map/reduce_scatter | solution.py:165
  50.6 19.8 %collective-permute-start.2 = (bf16[768,1024]{1,0:T(8,128)(2,1)S(1)}, bf16[768,1024]{1,0:T(8,128)(2,1)S(1)}, u32[]{:S(2)}, u32[]{:S(2)}) collective-permute-start(bf16[768,1024]{1,0:T(8,128)(2,1)S(1)} %collective-permute-done.1), channel_id=1, source_target_pairs={{0,1},{1,2},{2,3},{3,0},{4,5},{5,6},{6,7},{7,4},{8,9},{9,10},{10,1... | collective-permute-start | bytes 4718600 | tf_op jit(solution)/shard_map/ppermute | solution.py:133
  51.2 65.8 %copy-start.8 = (f32[768,64]{0,1:T(8,128)}, f32[768,64]{0,1:T(8,128)S(1)}, u32[]{:S(2)}) copy-start(f32[768,64]{0,1:T(8,128)S(1)} %get-tuple-element.25) | copy-start | bytes 589828
  51.2 65.9 %copy-start.6 = (f32[768,64]{0,1:T(8,128)}, f32[768,64]{0,1:T(8,128)S(1)}, u32[]{:S(2)}) copy-start(f32[768,64]{0,1:T(8,128)S(1)} %get-tuple-element.24) | copy-start | bytes 589828
  54.1 16.8 %copy-start = (bf16[768,1024]{1,0:T(8,128)(2,1)S(1)}, bf16[768,1024]{1,0:T(8,128)(2,1)}, u32[]{:S(2)}) copy-start(bf16[768,1024]{1,0:T(8,128)(2,1)} %param.11) | copy-start | bytes 4718596
  71.5 6.0 %copy-start.15 = (f32[4096]{0:T(1024)S(1)}, f32[4096]{0:T(1024)}, u32[]{:S(2)}) copy-start(f32[4096]{0:T(1024)} %param.12) | copy-start | bytes 49156
  71.7 4.5 %copy-start.1 = (bf16[768,8192]{1,0:T(8,128)(2,1)}, bf16[768,8192]{1,0:T(8,128)(2,1)S(1)}, u32[]{:S(2)}) copy-start(bf16[768,8192]{1,0:T(8,128)(2,1)S(1)} %constant_dynamic-update-slice_fusion) | copy-start | bytes 37748740
  77.5 83.5 %copy-start.11 = (f32[768]{0:T(1024)}, f32[768]{0:T(1024)S(1)}, u32[]{:S(2)}) copy-start(f32[768]{0:T(1024)S(1)} %add_rsqrt_fusion.2) | copy-start | bytes 9220
  82.8 87.5 %collective-permute-start.3 = (bf16[8,256]{1,0:T(8,128)(2,1)S(1)}, bf16[8,256]{1,0:T(8,128)(2,1)S(1)}, u32[]{:S(2)}, u32[]{:S(2)}) collective-permute-start(bf16[8,256]{1,0:T(8,128)(2,1)S(1)} %get-tuple-element.22), channel_id=1, source_target_pairs={{0,4},{4,8},{8,12},{12,16},{16,20},{20,24},{24,28},{1,5},{5,9},{9,... | collective-permute-start | bytes 12296 | tf_op jit(solution)/shard_map/ppermute | solution.py:21
  87.0 29.7 %copy-start.13 = (f32[64]{0:T(128)S(1)}, f32[64]{0:T(128)}, u32[]{:S(2)}) copy-start(f32[64]{0:T(128)} %param.18) | copy-start | bytes 772
  87.1 83.3 %collective-permute-start.4 = (bf16[8,256]{1,0:T(8,128)(2,1)S(1)}, bf16[8,256]{1,0:T(8,128)(2,1)S(1)}, u32[]{:S(2)}, u32[]{:S(2)}) collective-permute-start(bf16[8,256]{1,0:T(8,128)(2,1)S(1)} %get-tuple-element.23), channel_id=1, source_target_pairs={{4,0},{8,4},{12,8},{16,12},{20,16},{24,20},{28,24},{5,1},{9,5},{13... | collective-permute-start | bytes 12296 | tf_op jit(solution)/shard_map/ppermute | solution.py:24
  166.6 7.5 %collective-permute-start.5 = (bf16[128,512]{0,1:T(8,128)(2,1)S(1)}, bf16[128,512]{0,1:T(8,128)(2,1)S(1)}, u32[]{:S(2)}, u32[]{:S(2)}) collective-permute-start(bf16[128,512]{0,1:T(8,128)(2,1)S(1)} %get-tuple-element.16), channel_id=1, source_target_pairs={{0,4},{4,8},{8,12},{12,16},{16,20},{20,24},{24,28},{1,5},{5,9},{9,... | collective-permute-start | bytes 393224 | tf_op jit(solution)/shard_map/ppermute | solution.py:21
  169.0 10.7 %collective-permute-start.6 = (bf16[128,512]{0,1:T(8,128)(2,1)S(1)}, bf16[128,512]{0,1:T(8,128)(2,1)S(1)}, u32[]{:S(2)}, u32[]{:S(2)}) collective-permute-start(bf16[128,512]{0,1:T(8,128)(2,1)S(1)} %get-tuple-element.17), channel_id=1, source_target_pairs={{4,0},{8,4},{12,8},{16,12},{20,16},{24,20},{28,24},{5,1},{9,5},{13... | collective-permute-start | bytes 393224 | tf_op jit(solution)/shard_map/ppermute | solution.py:24
  181.0 55.2 %copy-start.12 = (f32[768]{0:T(1024)S(1)}, f32[768]{0:T(1024)}, u32[]{:S(2)}) copy-start(f32[768]{0:T(1024)} %copy-done.11) | copy-start | bytes 9220
  183.5 60.5 %copy-start.14 = (f32[64]{0:T(128)S(1)}, f32[64]{0:T(128)}, u32[]{:S(2)}) copy-start(f32[64]{0:T(128)} %param.17) | copy-start | bytes 772
  244.0 1.0 copy-start.9
  244.0 1.1 copy-start.7
  244.9 1.4 copy-start.2
  248.2 2.5 copy-start.10
  311.3 50.5 %copy-start.3 = (f32[1,768,256]{2,1,0:T(8,128)S(1)}, f32[1,768,256]{2,1,0:T(8,128)}, u32[]{:S(2)}) copy-start(f32[1,768,256]{2,1,0:T(8,128)} %get-tuple-element.40) | copy-start | bytes 2359300
  311.3 50.5 %copy-start.4 = (f32[1,768,256]{2,1,0:T(8,128)S(1)}, f32[1,768,256]{2,1,0:T(8,128)}, u32[]{:S(2)}) copy-start(f32[1,768,256]{2,1,0:T(8,128)} %get-tuple-element.41) | copy-start | bytes 2359300
  311.3 50.5 %copy-start.5 = (f32[1,768,256]{2,1,0:T(8,128)S(1)}, f32[1,768,256]{2,1,0:T(8,128)}, u32[]{:S(2)}) copy-start(f32[1,768,256]{2,1,0:T(8,128)} %get-tuple-element.38) | copy-start | bytes 2359300
Sparse Core Ops, SparseCore 0:
  9.5 51.7 all-gather.6
  63.4 47.6 all-gather.10
  113.3 47.6 all-gather.12
  162.9 73.2 all-gather.14
  238.1 73.1 all-gather.16
  313.2 48.5 all-gather.8
  371.6 57.2 reduce-scatter.1
